TPU v7x, 32 devices: a whole 2x2x4 slice. The times are simulated.
32 devices in a mesh: rep: 4 (over z), fs: 4 (over y, x), tp: 2 (over core).
Axes of the slice: x: 2, y: 2, z: 4, core: 2. Of those that a mesh axis runs over, the one named last changes fastest.
Arguments:
- tokens: bfloat16 [2048, 1024], P(('rep', 'fs', 'tp')), may hold values from -6 to 6
- cotangent: bfloat16 [2048, 1024], P(('rep', 'fs', 'tp')), may hold values from -6 to 6
- gate_weight: bfloat16 [1024, 2816], P('fs', 'tp'), may hold values from -0.1875 to 0.1875
- up_weight: bfloat16 [1024, 2816], P('fs', 'tp'), may hold values from -0.1875 to 0.1875
- down_weight: bfloat16 [2816, 1024], P('tp', 'fs'), may hold values from -0.109375 to 0.109375
Outputs:
- input_grad: bfloat16 [2048, 1024], P(('rep', 'fs', 'tp'))
- gate_grad: float32 [1024, 2816], P('fs', 'tp')
- up_grad: float32 [1024, 2816], P('fs', 'tp')
- down_grad: float32 [2816, 1024], P('tp', 'fs')
- gate_power: float32 [1024], P('fs')
- up_power: float32 [1024], P('fs')
- down_power: float32 [2816], P('tp')
All inputs are finite; a program needn't handle non-finite values.
Results may differ from a plain program's by a relative error of at most 0.0017.
Values may be sent and summed in bfloat16 or wider, within the bound.
A program may use at most 64 MiB of HBM per device.

v0:
```python
import math
import jax
import jax.numpy as jnp
from jax import lax
from jax.sharding import PartitionSpec as P

D = 1024
FF = 2816
EPSILON = 1e-06


def contract_rows(left, right):
    return lax.dot_general(
        left, right, (((0,), (0,)), ((), ())), preferred_element_type=jnp.float32
    )


def contract_cols(left, right):
    return lax.dot_general(
        left, right, (((1,), (1,)), ((), ())), preferred_element_type=jnp.float32
    )


def on_device(tokens, cotangent, gate_weight, up_weight, down_weight):
    tp_count = lax.axis_size("tp")
    fs_count = lax.axis_size("fs")
    rep_count = lax.axis_size("rep")
    width = tokens.shape[1]
    factor = 1.0 / math.sqrt(tokens.shape[0] * tp_count * fs_count * rep_count)
    xfloat = tokens.astype(jnp.float32)
    recip_norm = lax.rsqrt(jnp.mean(xfloat * xfloat, axis=1, keepdims=True) + EPSILON)
    normed_exact = xfloat * recip_norm
    normed = normed_exact.astype(jnp.bfloat16)
    group_normed, group_cotangent = (
        lax.all_gather(normed, "tp", axis=0, tiled=True),
        lax.all_gather(cotangent, "tp", axis=0, tiled=True),
    )
    gate_full, up_full, down_full = (
        lax.all_gather(gate_weight, "fs", axis=0, tiled=True),
        lax.all_gather(up_weight, "fs", axis=0, tiled=True),
        lax.all_gather(down_weight.T, "fs", axis=0, tiled=True),
    )
    gate_pre = jnp.dot(group_normed, gate_full, preferred_element_type=jnp.float32)
    up_pre = jnp.dot(group_normed, up_full, preferred_element_type=jnp.float32)
    sigmoid_gate = jax.nn.sigmoid(gate_pre)
    activated = gate_pre * sigmoid_gate
    hidden = (activated * up_pre).astype(jnp.bfloat16)
    grad_hidden = 0.5 * jnp.dot(group_cotangent, down_full, preferred_element_type=jnp.float32)
    grad_up_pre = (grad_hidden * activated).astype(jnp.bfloat16)
    grad_gate_pre = (
        grad_hidden * up_pre * sigmoid_gate * (1.0 + gate_pre * (1.0 - sigmoid_gate))
    ).astype(jnp.bfloat16)
    normed_part = contract_cols(grad_gate_pre, gate_full) + contract_cols(grad_up_pre, up_full)
    grad_normed = lax.psum_scatter(normed_part, "tp", scatter_dimension=0, tiled=True)
    inner = jnp.mean(grad_normed * normed_exact, axis=1, keepdims=True)
    input_grad = (recip_norm * (grad_normed - normed_exact * inner)).astype(jnp.bfloat16)
    hidden_local = gate_weight.shape[1]

    def rows_term():
        normed_cols = lax.slice_in_dim(
            group_normed, 0, width // fs_count * lax.axis_size("fs"), axis=1
        )
        cotangent_cols = lax.slice_in_dim(
            group_cotangent, 0, width // fs_count * lax.axis_size("fs"), axis=1
        )
        return factor * jnp.concatenate(
            [
                contract_rows(normed_cols, grad_gate_pre),
                contract_rows(normed_cols, grad_up_pre),
                0.5 * contract_rows(cotangent_cols, hidden),
            ],
            axis=1,
        )

    reduced = lax.psum_scatter(rows_term(), "fs", scatter_dimension=0, tiled=True)
    reduced = lax.psum(reduced, "rep")
    gate_grad = reduced[:, :hidden_local]
    up_grad = reduced[:, hidden_local : 2 * hidden_local]
    down_grad = reduced[:, 2 * hidden_local :].T
    gate_sums, up_sums = lax.psum(
        (jnp.sum(gate_grad * gate_grad, axis=1), jnp.sum(up_grad * up_grad, axis=1)), "tp"
    )
    down_sums = lax.psum(jnp.sum(down_grad * down_grad, axis=1), "fs")
    return (input_grad, gate_grad, up_grad, down_grad, gate_sums / FF, up_sums / FF, down_sums / D)


def solution(mesh):
    placed = (
        P(("rep", "fs", "tp"), None),
        P(("rep", "fs", "tp"), None),
        P("fs", "tp"),
        P("fs", "tp"),
        P("tp", "fs"),
    )
    return jax.shard_map(
        on_device,
        mesh=mesh,
        in_specs=placed,
        out_specs=(
            P(("rep", "fs", "tp"), None),
            P("fs", "tp"),
            P("fs", "tp"),
            P("tp", "fs"),
            P("fs"),
            P("fs"),
            P("tp"),
        ),
        check_vma=False,
    )
```

profile of v0, /device:TPU:0, one launch (start us, length us, event | category | flops | bytes accessed | tf_op | source)
XLA Modules:
  0.0 513.0 jit_solution(5771994517067918810)
XLA Ops:
  7.2 0.0 all-gather.8.cloned.1.call-start
  7.2 0.7 all-gather.8.cloned.1.call-update
  7.9 0.0 all-gather.6.cloned.1.call-start
  8.0 0.7 all-gather.6.cloned.1.call-update
  8.7 0.0 all-gather.4.cloned.1.call-start
  8.7 0.7 all-gather.4.cloned.1.call-update
  9.4 0.0 reduce-scatter.5.cloned.1.call-start
  9.4 1.0 fusion.8
  10.5 1.0 fusion.3
  11.5 2.1 all_gather.17
  13.6 2.0 all_gather.15
  15.6 38.7 %all-gather.8.cloned.1.call-done = bf16[1024,1408]{1,0:T(8,128)(2,1)} async-done(((bf16[256,1408]{1,0:T(8,128)(2,1)}), bf16[1024,1408]{1,0:T(8,128)(2,1)}) %all-gather.8.cloned.1.call-update) | async-done | bytes 2883600 | tf_op jit(solution)/shard_map/all_gather | solution.py:39
  54.3 2.4 fusion.12
  56.7 41.1 %all-gather.6.cloned.1.call-done = bf16[1024,1408]{1,0:T(8,128)(2,1)} async-done(((bf16[256,1408]{1,0:T(8,128)(2,1)}), bf16[1024,1408]{1,0:T(8,128)(2,1)}) %all-gather.6.cloned.1.call-update) | async-done | bytes 2883600 | tf_op jit(solution)/shard_map/all_gather | solution.py:40
  97.8 2.4 fusion.11
  100.2 3.5 multiply_bitcast_fusion
  103.7 37.5 %all-gather.4.cloned.1.call-done = bf16[1024,1408]{0,1:T(8,128)(2,1)} async-done(((bf16[256,1408]{0,1:T(8,128)(2,1)}), bf16[1024,1408]{0,1:T(8,128)(2,1)}) %all-gather.4.cloned.1.call-update) | async-done | bytes 2883600 | tf_op jit(solution)/shard_map/all_gather | solution.py:41
  141.2 2.9 multiply_convert_fusion.1
  144.1 0.0 copy-start.3
  144.2 0.9 fusion.15
  145.1 0.0 slice-start
  145.1 0.0 slice-start.1
  145.1 0.9 fusion.14
  146.1 1.2 slice-done
  147.3 0.5 slice-done.1
  147.8 6.3 %maximum_multiply_fusion = f32[1024,4224]{1,0:T(8,128)} fusion(f32[1024,1408]{1,0:T(8,128)S(1)} %bitcast.23, f32[1024,1408]{1,0:T(8,128)S(1)} %fusion.15, f32[1024,1408]{1,0:T(8,128)S(1)} %fusion.14), kind=kLoop, calls=%fused_computation | loop fusion | flops 12976128 | bytes 34603008 | tf_op jit(solution)/shard_map/mul | solution.py:66
  154.1 0.0 reduce-scatter.5.cloned.1.call-update
  154.1 0.0 reduce-scatter.3.cloned.1.call-start
  154.2 1.7 copy-done
  155.9 1.0 fusion.13
  157.0 0.8 copy-done.1
  157.7 0.0 copy-done.4
  157.7 1.8 convolution_add_fusion
  159.6 0.0 reduce-scatter.3.cloned.1.call-update
  159.6 0.0 all-reduce.3.cloned.1.call-start
  159.7 152.6 %reduce-scatter.5.cloned.1.call-done = f32[256,4224]{1,0:T(8,128)} async-done(((f32[1024,4224]{1,0:T(8,128)}), f32[256,4224]{1,0:T(8,128)}) %reduce-scatter.5.cloned.1.call-update) | async-done | bytes 4325392 | tf_op jit(solution)/shard_map/reduce_scatter | solution.py:75
  312.3 0.0 all-reduce.3.cloned.1.call-update
  312.3 10.6 %reduce-scatter.3.cloned.1.call-done = f32[64,1024]{1,0:T(8,128)} async-done(((f32[128,1024]{1,0:T(8,128)}), f32[64,1024]{1,0:T(8,128)}) %reduce-scatter.3.cloned.1.call-update) | async-done | bytes 262160 | tf_op jit(solution)/shard_map/reduce_scatter | solution.py:54
  322.9 1.2 fusion.4
  324.0 1.7 fusion.7
  325.8 159.7 %all-reduce.3.cloned.1.call-done = f32[256,4224]{1,0:T(8,128)} async-done(((f32[256,4224]{1,0:T(8,128)}), f32[256,4224]{1,0:T(8,128)}) %all-reduce.3.cloned.1.call-update) | async-done | bytes 4325392 | tf_op jit(solution)/shard_map/psum | solution.py:76
  485.5 1.5 multiply_reduce_fusion
  487.0 10.1 %psum.31 = f32[1408]{0:T(1024)S(1)} all-reduce(f32[1408]{0:T(1024)S(1)} %multiply_reduce_fusion), channel_id=1, replica_groups=mesh['rep'=4,'fs'=4,'tp'=2] {'fs'}, use_global_device_ids=true, to_apply=%region_10.0 | all-reduce | flops 1408 | bytes 11264 | tf_op jit(solution)/shard_map/psum | solution.py:83
  497.0 0.6 broadcast_multiply_fusion
  497.6 3.9 multiply_reduce_fusion.1
  501.6 1.5 copy.13
  503.1 2.4 all-reduce
  505.5 0.6 broadcast_multiply_fusion.1
  (11 shorter events, 0.0 us)
Async XLA Ops:
  7.2 6.5 %copy-start.5 = (bf16[64,1024]{1,0:T(8,128)(2,1)S(1)}, bf16[64,1024]{1,0:T(8,128)(2,1)}, u32[]{:S(2)}) copy-start(bf16[64,1024]{1,0:T(8,128)(2,1)} %param.6) | copy-start | bytes 393220
  7.2 47.1 %all-gather.8.cloned.1.call-start = ((), (), s32[]{:S(2)}) async-start(), calls=%async_computation.4 | async-start | bytes 3604480 | tf_op jit(solution)/shard_map/all_gather | solution.py:39
  7.9 89.9 %all-gather.6.cloned.1.call-start = ((), (), s32[]{:S(2)}) async-start(), calls=%async_computation.3 | async-start | bytes 3604480 | tf_op jit(solution)/shard_map/all_gather | solution.py:40
  8.7 132.5 %all-gather.4.cloned.1.call-start = ((), (), s32[]{:S(2)}) async-start(), calls=%async_computation.2 | async-start | bytes 3604480 | tf_op jit(solution)/shard_map/all_gather | solution.py:41
  9.4 302.9 %reduce-scatter.5.cloned.1.call-start = ((), (), s32[]{:S(2)}) async-start(), calls=%async_computation.6 | async-start | bytes 21626880 | tf_op jit(solution)/shard_map/reduce_scatter | solution.py:75
  144.1 1.0 copy-start.3
  145.1 2.2 slice-start
  145.1 2.7 slice-start.1
  154.1 1.8 copy-start
  154.1 168.8 %reduce-scatter.3.cloned.1.call-start = ((), (), s32[]{:S(2)}) async-start(), calls=%async_computation.5 | async-start | bytes 786432 | tf_op jit(solution)/shard_map/reduce_scatter | solution.py:54
  155.9 1.8 copy-start.1
  155.9 1.8 copy-start.4
  159.6 163.3 %copy-start.2 = (bf16[64,1024]{1,0:T(8,128)(2,1)S(1)}, bf16[64,1024]{1,0:T(8,128)(2,1)}, u32[]{:S(2)}) copy-start(bf16[64,1024]{1,0:T(8,128)(2,1)} %param.5) | copy-start | bytes 393220
  159.6 325.9 %all-reduce.3.cloned.1.call-start = ((), (), s32[]{:S(2)}) async-start(), calls=%async_computation.7 | async-start | bytes 8650752 | tf_op jit(solution)/shard_map/psum | solution.py:76
Sparse Core Ops, SparseCore 0:
  9.8 44.3 all-gather.7
  56.1 41.6 all-gather.5
  99.6 41.5 all-gather.3
  154.2 157.9 reduce-scatter.4
  314.9 7.9 reduce-scatter.2
  325.1 160.3 all-reduce.2
where the time goes:
time: 513 us
  waiting for transfers between devices  442 us (86%)
  other arithmetic  17.8 us (3%)
  blocking collectives  16.6 us (3%)
  matrix products  16 us (3%)
  between operations  14.2 us (3%)
  local copies, waits for them, and re-layouts  5.81 us (1%)
    psum x1, waiting for transfers between devices, on_device(): reduced = lax.psum(reduced, 'rep')  160 us
    reduce_scatter x1, waiting for transfers between devices, on_device(): lax.psum_scatter(rows_term(), 'fs', scatter_dimension=0, tiled=True)  153 us
    all_gather x1, waiting for transfers between devices, on_device(): lax.all_gather(up_weight, 'fs', axis=0, tiled=True)  41.1 us
    all_gather x1, waiting for transfers between devices, on_device(): lax.all_gather(gate_weight, 'fs', axis=0, tiled=True)  38.7 us
    all_gather x1, waiting for transfers between devices, on_device(): lax.all_gather(down_weight.T, 'fs', axis=0, tiled=True)  37.5 us
    reduce_scatter x1, waiting for transfers between devices, on_device(): lax.psum_scatter(normed_part, 'tp', scatter_dimension=0, tiled=True)  10.6 us
  transfers between devices with their start and end apart: 6, of which 6 were waited for; matrix products, arithmetic and copies ran while one was open for 3% of the time, Pallas kernels for 0%

commit v1 on v0

--- a/solution.py
+++ b/solution.py
@@ -73,7 +73,9 @@
         )
 
     reduced = lax.psum_scatter(rows_term(), "fs", scatter_dimension=0, tiled=True)
-    reduced = lax.psum(reduced, "rep")
+    reduced = reduced
+    for hop in (1, 2):
+        reduced = reduced + lax.ppermute(reduced, "rep", [(dev, dev ^ hop) for dev in range(4)])
     gate_grad = reduced[:, :hidden_local]
     up_grad = reduced[:, hidden_local : 2 * hidden_local]
     down_grad = reduced[:, 2 * hidden_local :].T

time: 513 us -> 628 us (1.22)
  waiting for transfers between devices: 442 us -> 551 us
    ppermute x0 -> x2, waiting for transfers between devices: none -> 267 us  [on_device(): lax.ppermute(reduced, 'rep', [(dev, dev ^ hop) for dev in range(4)])]
    psum x1 -> x0, waiting for transfers between devices: 160 us -> none  [on_device(): reduced = lax.psum(reduced, 'rep')]
    add x0 -> x2, other arithmetic: none -> 8.81 us  [on_device(): reduced + lax.ppermute(reduced, 'rep', [(dev, dev ^ hop) for dev in range...]
  transfers between devices with their start and end apart: 6 -> 7, of which waited for: 6 -> 7; matrix products, arithmetic and copies ran while one was open for 3% -> 3% of each run, Pallas kernels for 0% -> 0%
where the time goes in v1:
time: 628 us; the launch traced here: 627 us
  waiting for transfers between devices  551 us (88%)
  other arithmetic  23.3 us (4%)
  matrix products  15.9 us (3%)
  blocking collectives  15.6 us (2%)
  between operations  13.9 us (2%)
    ppermute x2, waiting for transfers between devices, on_device(): lax.ppermute(reduced, 'rep', [(dev, dev ^ hop) for dev in range(4)])  267 us
    reduce_scatter x1, waiting for transfers between devices, on_device(): lax.psum_scatter(rows_term(), 'fs', scatter_dimension=0, tiled=True)  158 us
    all_gather x1, waiting for transfers between devices, on_device(): lax.all_gather(up_weight, 'fs', axis=0, tiled=True)  41.1 us
    all_gather x1, waiting for transfers between devices, on_device(): lax.all_gather(gate_weight, 'fs', axis=0, tiled=True)  38.7 us
    all_gather x1, waiting for transfers between devices, on_device(): lax.all_gather(down_weight.T, 'fs', axis=0, tiled=True)  37.5 us
  transfers between devices with their start and end apart: 7, of which 7 were waited for; matrix products, arithmetic and copies ran while one was open for 3% of the time, Pallas kernels for 0%

profile of v1, /device:TPU:0, one launch (start us, length us, event | category | flops | bytes accessed | tf_op | source)
XLA Modules:
  0.0 627.1 jit_solution(7118076766176071614)
XLA Ops:
  7.2 0.0 all-gather.8.cloned.1.call-start
  7.2 0.7 all-gather.8.cloned.1.call-update
  7.9 0.0 all-gather.6.cloned.1.call-start
  8.0 0.7 all-gather.6.cloned.1.call-update
  8.7 0.0 all-gather.4.cloned.1.call-start
  8.7 0.7 all-gather.4.cloned.1.call-update
  9.4 0.0 reduce-scatter.5.cloned.1.call-start
  9.4 1.0 fusion.8
  10.5 1.0 fusion.3
  11.5 2.1 all_gather.17
  13.6 2.0 all_gather.15
  15.6 38.7 %all-gather.8.cloned.1.call-done = bf16[1024,1408]{1,0:T(8,128)(2,1)} async-done(((bf16[256,1408]{1,0:T(8,128)(2,1)}), bf16[1024,1408]{1,0:T(8,128)(2,1)}) %all-gather.8.cloned.1.call-update) | async-done | bytes 2883600 | tf_op jit(solution)/shard_map/all_gather | solution.py:39
  54.3 2.4 fusion.12
  56.7 41.1 %all-gather.6.cloned.1.call-done = bf16[1024,1408]{1,0:T(8,128)(2,1)} async-done(((bf16[256,1408]{1,0:T(8,128)(2,1)}), bf16[1024,1408]{1,0:T(8,128)(2,1)}) %all-gather.6.cloned.1.call-update) | async-done | bytes 2883600 | tf_op jit(solution)/shard_map/all_gather | solution.py:40
  97.8 2.4 fusion.11
  100.2 3.5 multiply_bitcast_fusion
  103.7 37.5 %all-gather.4.cloned.1.call-done = bf16[1024,1408]{0,1:T(8,128)(2,1)} async-done(((bf16[256,1408]{0,1:T(8,128)(2,1)}), bf16[1024,1408]{0,1:T(8,128)(2,1)}) %all-gather.4.cloned.1.call-update) | async-done | bytes 2883600 | tf_op jit(solution)/shard_map/all_gather | solution.py:41
  141.2 2.9 multiply_convert_fusion.1
  144.1 0.0 copy-start.3
  144.2 0.9 fusion.15
  145.1 0.0 slice-start
  145.1 0.9 fusion.14
  146.1 1.2 slice-done
  147.3 0.5 slice-done.1
  147.8 6.3 %maximum_multiply_fusion = f32[1024,4224]{1,0:T(8,128)} fusion(f32[1024,1408]{1,0:T(8,128)S(1)} %bitcast.23, f32[1024,1408]{1,0:T(8,128)S(1)} %fusion.15, f32[1024,1408]{1,0:T(8,128)S(1)} %fusion.14), kind=kLoop, calls=%fused_computation | loop fusion | flops 12976128 | bytes 34603008 | tf_op jit(solution)/shard_map/mul | solution.py:66
  154.1 0.0 reduce-scatter.5.cloned.1.call-update
  154.1 0.0 reduce-scatter.3.cloned.1.call-start
  154.2 158.1 %reduce-scatter.5.cloned.1.call-done = f32[256,4224]{1,0:T(8,128)} async-done(((f32[1024,4224]{1,0:T(8,128)}), f32[256,4224]{1,0:T(8,128)}) %reduce-scatter.5.cloned.1.call-update) | async-done | bytes 4325392 | tf_op jit(solution)/shard_map/reduce_scatter | solution.py:75
  312.3 1.5 collective-permute-start
  313.8 93.7 %collective-permute-done = f32[256,4224]{1,0:T(8,128)S(1)} collective-permute-done((f32[256,4224]{1,0:T(8,128)}, f32[256,4224]{1,0:T(8,128)S(1)}, u32[]{:S(2)}, u32[]{:S(2)}) %collective-permute-start) | collective-permute-done | bytes 4325408 | tf_op jit(solution)/shard_map/ppermute | solution.py:78
  407.4 4.8 add.41
  412.3 2.4 collective-permute-start.1
  414.7 1.0 fusion.13
  415.7 0.0 copy-start.2
  415.7 1.9 convolution_add_fusion
  417.6 0.0 reduce-scatter.3.cloned.1.call-update
  417.6 6.5 %reduce-scatter.3.cloned.1.call-done = f32[64,1024]{1,0:T(8,128)} async-done(((f32[128,1024]{1,0:T(8,128)}), f32[64,1024]{1,0:T(8,128)}) %reduce-scatter.3.cloned.1.call-update) | async-done | bytes 262160 | tf_op jit(solution)/shard_map/reduce_scatter | solution.py:54
  424.1 1.2 fusion.4
  425.2 1.7 fusion.7
  427.0 173.3 %collective-permute-done.1 = f32[256,4224]{1,0:T(8,128)} collective-permute-done((f32[256,4224]{1,0:T(8,128)}, f32[256,4224]{1,0:T(8,128)}, u32[]{:S(2)}, u32[]{:S(2)}) %collective-permute-start.1) | collective-permute-done | bytes 4325408 | tf_op jit(solution)/shard_map/ppermute | solution.py:78
  600.3 4.0 add.42
  604.3 0.1 multiply_reduce_fusion
  604.4 2.0 multiply_reduce_fusion.1
  606.4 9.0 %psum.23 = f32[1408]{0:T(1024)S(1)} all-reduce(f32[1408]{0:T(1024)S(1)} %multiply_reduce_fusion), channel_id=1, replica_groups=mesh['rep'=4,'fs'=4,'tp'=2] {'fs'}, use_global_device_ids=true, to_apply=%region_9.0 | all-reduce | flops 1408 | bytes 11264 | tf_op jit(solution)/shard_map/psum | solution.py:85
  615.4 0.6 broadcast_multiply_fusion
  616.0 1.5 copy.13
  617.5 2.4 all-reduce
  620.0 0.6 broadcast_multiply_fusion.1
  (14 shorter events, 0.0 us)
Async XLA Ops:
  7.2 6.5 %copy-start.5 = (bf16[64,1024]{1,0:T(8,128)(2,1)S(1)}, bf16[64,1024]{1,0:T(8,128)(2,1)}, u32[]{:S(2)}) copy-start(bf16[64,1024]{1,0:T(8,128)(2,1)} %param.6) | copy-start | bytes 393220
  7.2 47.1 %all-gather.8.cloned.1.call-start = ((), (), s32[]{:S(2)}) async-start(), calls=%async_computation.4 | async-start | bytes 3604480 | tf_op jit(solution)/shard_map/all_gather | solution.py:39
  7.9 89.9 %all-gather.6.cloned.1.call-start = ((), (), s32[]{:S(2)}) async-start(), calls=%async_computation.3 | async-start | bytes 3604480 | tf_op jit(solution)/shard_map/all_gather | solution.py:40
  8.7 132.5 %all-gather.4.cloned.1.call-start = ((), (), s32[]{:S(2)}) async-start(), calls=%async_computation.2 | async-start | bytes 3604480 | tf_op jit(solution)/shard_map/all_gather | solution.py:41
  9.4 302.9 %reduce-scatter.5.cloned.1.call-start = ((), (), s32[]{:S(2)}) async-start(), calls=%async_computation.6 | async-start | bytes 21626880 | tf_op jit(solution)/shard_map/reduce_scatter | solution.py:75
  144.1 1.0 copy-start.3
  145.1 2.2 slice-start
  145.1 2.7 slice-start.1
  154.1 260.5 %copy-start = (bf16[1024,1408]{1,0:T(8,128)(2,1)S(1)}, bf16[1024,1408]{1,0:T(8,128)(2,1)}, u32[]{:S(2)}) copy-start(bf16[1024,1408]{1,0:T(8,128)(2,1)} %all-gather.8.cloned.1.call-done) | copy-start | bytes 8650756
  154.1 269.9 %reduce-scatter.3.cloned.1.call-start = ((), (), s32[]{:S(2)}) async-start(), calls=%async_computation.5 | async-start | bytes 786432 | tf_op jit(solution)/shard_map/reduce_scatter | solution.py:54
  312.3 95.2 %collective-permute-start = (f32[256,4224]{1,0:T(8,128)}, f32[256,4224]{1,0:T(8,128)S(1)}, u32[]{:S(2)}, u32[]{:S(2)}) collective-permute-start(f32[256,4224]{1,0:T(8,128)} %reduce-scatter.5.cloned.1.call-done), channel_id=1, source_target_pairs={{0,8},{8,0},{16,24},{24,16},{1,9},{9,1},{17,25},{25,17},{2,10},{10... | collective-permute-start | bytes 12976136 | tf_op jit(solution)/shard_map/ppermute | solution.py:78
  412.3 3.4 copy-start.1
  412.3 3.4 copy-start.4
  412.3 188.0 %collective-permute-start.1 = (f32[256,4224]{1,0:T(8,128)}, f32[256,4224]{1,0:T(8,128)}, u32[]{:S(2)}, u32[]{:S(2)}) collective-permute-start(f32[256,4224]{1,0:T(8,128)} %add.41), channel_id=1, source_target_pairs={{0,16},{8,24},{16,0},{24,8},{1,17},{9,25},{17,1},{25,9},{2,18},{10... | collective-permute-start | bytes 12976136 | tf_op jit(solution)/shard_map/ppermute | solution.py:78
  415.7 8.3 %copy-start.2 = (bf16[64,1024]{1,0:T(8,128)(2,1)S(1)}, bf16[64,1024]{1,0:T(8,128)(2,1)}, u32[]{:S(2)}) copy-start(bf16[64,1024]{1,0:T(8,128)(2,1)} %param.5) | copy-start | bytes 393220
Sparse Core Ops, SparseCore 0:
  9.8 44.3 all-gather.7
  56.1 41.6 all-gather.5
  99.6 41.5 all-gather.3
  154.2 157.9 reduce-scatter.4
  417.7 6.2 reduce-scatter.2
